TPU v7x, 32 devices: a whole 2x2x4 slice. The times are simulated.
32 devices in a mesh: sp: 16 (over z, y, x), tp: 2 (over core).
Axes of the slice: x: 2, y: 2, z: 4, core: 2. Of those that a mesh axis runs over, the one named last changes fastest.
Arguments:
- query_one: bfloat16 [2048, 1024], P('sp', 'tp'), may hold values from -6 to 6
- key_one: bfloat16 [2048, 1024], P('sp', 'tp'), may hold values from -6 to 6
- query_two: bfloat16 [2048, 512], P('sp', 'tp'), may hold values from -6 to 6
- key_two: bfloat16 [2048, 512], P('sp', 'tp'), may hold values from -6 to 6
- values: bfloat16 [2048, 2048], P('sp', 'tp'), may hold values from -6 to 6
- out_gate: bfloat16 [2048, 2048], P('sp', 'tp'), may hold values from -6 to 6
- in_gate: float32 [16, 2048], P('tp', 'sp'), may hold values from -3 to 150
- forget_gate: float32 [16, 2048], P('tp', 'sp'), may hold values from -1 to 24
- head_gain: float32 [2048], P('tp'), may hold values from 0.1 to 1.9
- out_weight: bfloat16 [2048, 2048], P('tp'), may hold values from -0.125 to 0.125
- stream: bfloat16 [2048, 2048], P('sp'), may hold values from -6 to 6
- mix_gain: float32 [2048], replicated, may hold values from 0.1 to 1.9
- up_weight: bfloat16 [2048, 8192], P('sp', 'tp'), may hold values from -0.125 to 0.125
- down_weight: bfloat16 [8192, 2048], P('tp', 'sp'), may hold values from -0.0625 to 0.0625
- out_gain: float32 [2048], replicated, may hold values from 0.1 to 1.9
Outputs:
- result: bfloat16 [2048, 2048], P(('sp', 'tp'))
All inputs are finite; a program needn't handle non-finite values.
Results may differ from a plain program's by a relative error of at most 0.018.
Values may be sent and summed in bfloat16 or wider, within the bound.
A program may use at most 128 MiB of HBM per device.

v0:
```python
from functools import partial
import jax
import jax.numpy as jnp
from jax import lax
from jax.sharding import PartitionSpec as P

BLOCK = 64
NEG_BIG = -1e30
EPS = 1e-05


def prefix_2(part, axis, combine, identity):
    place = lax.axis_index(axis)
    gathered = jax.tree.map(lambda a: lax.all_gather(a, axis), part)
    state = jax.tree.map(lambda a, e: jnp.zeros_like(a) + jnp.asarray(e, a.dtype), part, identity)

    def one(lap, state):
        return combine(
            state, jax.tree.map(lambda a: lax.dynamic_index_in_dim(a, lap, 0, False), gathered)
        )

    return lax.fori_loop(0, place, one, state)


def combine(earlier, later):
    decay_early, cell_early, norm_early, peak_early = earlier
    decay_late, cell_late, norm_late, peak_late = later
    ceiling = jnp.maximum(decay_late + peak_early, peak_late)
    keep_share = jnp.exp(decay_late + peak_early - ceiling)
    fresh_share = jnp.exp(peak_late - ceiling)
    cell_new = keep_share[..., None, None] * cell_early + fresh_share[..., None, None] * cell_late
    norm_new = keep_share[..., None] * norm_early + fresh_share[..., None] * norm_late
    return (decay_early + decay_late, cell_new, norm_new, ceiling)


def combine_groups(earlier, later):
    return (combine(earlier[0], later[0]), combine(earlier[1], later[1]))


def summarize(queries, keys_in, values_in, in_pre, forget_pre, block_len):
    length, width_k = queries.shape
    block_count = length // block_len
    scaled_keys = keys_in.astype(jnp.float32).reshape(
        block_count, block_len, width_k
    ) * width_k ** (-0.5)
    values_f = values_in.astype(jnp.float32).reshape(block_count, block_len, -1)
    width_v = values_f.shape[-1]
    log_forget = jax.nn.log_sigmoid(forget_pre).reshape(block_count, block_len)
    log_input = in_pre.reshape(block_count, block_len)
    cumulative = jnp.cumsum(log_forget, 1)
    decay_total = cumulative[:, -1]
    weight_log = decay_total[:, None] - cumulative + log_input
    peak_log = jnp.max(weight_log, 1)
    weighted = jnp.exp(weight_log - peak_log[:, None])[..., None] * scaled_keys
    cell_states = jnp.einsum("cld,cle->cde", weighted, values_f, precision=lax.Precision.HIGHEST)
    norm_states = jnp.sum(weighted, 1)
    identity = (
        jnp.zeros((), jnp.float32),
        jnp.zeros((width_k, width_v), jnp.float32),
        jnp.zeros((width_k,), jnp.float32),
        jnp.full((), NEG_BIG, jnp.float32),
    )

    def advance(running, element):
        return (combine(running, element), running)

    closing, prefix = lax.scan(advance, identity, (decay_total, cell_states, norm_states, peak_log))
    return (closing, prefix, (scaled_keys, values_f, cumulative, log_input))


def finish(queries, prefix, pieces, incoming):
    scaled_keys, values_f, cumulative, log_input = pieces
    block_count, block_len, width_k = scaled_keys.shape
    spread_in = jax.tree.map(
        lambda leaf: jnp.broadcast_to(leaf, (block_count,) + leaf.shape), incoming
    )
    _, cell_states, norm_states, peaks = combine(spread_in, prefix)
    query_f = queries.astype(jnp.float32).reshape(block_count, block_len, width_k)
    log_gaps = cumulative[:, :, None] - cumulative[:, None, :] + log_input[:, None, :]
    causal = jnp.arange(block_len)[:, None] >= jnp.arange(block_len)[None, :]
    log_gaps = jnp.where(causal[None], log_gaps, -jnp.inf)
    carried = cumulative + peaks[:, None]
    ceiling = jnp.maximum(carried, jnp.max(log_gaps, 2))
    scores = jnp.einsum("cld,csd->cls", query_f, scaled_keys, precision=lax.Precision.HIGHEST)
    scores = scores * jnp.exp(log_gaps - ceiling[..., None])
    carry_weight = jnp.exp(carried - ceiling)
    numerator = carry_weight[..., None] * jnp.einsum(
        "cld,cde->cle", query_f, cell_states, precision=lax.Precision.HIGHEST
    )
    numerator = numerator + jnp.einsum(
        "cls,cse->cle", scores, values_f, precision=lax.Precision.HIGHEST
    )
    denominator = carry_weight * jnp.einsum(
        "cld,cd->cl", query_f, norm_states, precision=lax.Precision.HIGHEST
    )
    denominator = denominator + jnp.sum(scores, 2)
    result = numerator / jnp.maximum(jnp.abs(denominator), jnp.exp(-ceiling))[..., None]
    return result.reshape(block_count * block_len, -1)


def head_norm(cell_out):
    center = jnp.mean(cell_out, -1, keepdims=True)
    spread = jnp.mean(jnp.square(cell_out - center), -1, keepdims=True)
    return (cell_out - center) * lax.rsqrt(spread + EPS)


def layer_norm(rows_f, gain):
    center = jnp.mean(rows_f, -1, keepdims=True)
    spread = jnp.mean(jnp.square(rows_f - center), -1, keepdims=True)
    return (rows_f - center) * lax.rsqrt(spread + EPS) * gain


def empty_state(head_pairs, width_k, width_v):
    return (
        jnp.zeros((head_pairs,), jnp.float32),
        jnp.zeros((head_pairs, width_k, width_v), jnp.float32),
        jnp.zeros((head_pairs, width_k), jnp.float32),
        jnp.full((head_pairs,), NEG_BIG, jnp.float32),
    )


def body(
    query_one,
    key_one,
    query_two,
    key_two,
    values,
    out_gate,
    in_gate,
    forget_gate,
    head_gain,
    out_weight,
    stream,
    mix_gain,
    up_weight,
    down_weight,
    out_gain,
):
    length = stream.shape[0]
    head_pairs = in_gate.shape[0] // 2
    width_v = values.shape[1] // (2 * head_pairs)

    def split_heads(array):
        return array.reshape(length, head_pairs, -1).transpose(1, 0, 2)

    values_split = values.reshape(length, head_pairs, 2, width_v).transpose(1, 2, 0, 3)
    input_rows = in_gate.reshape(head_pairs, 2, length)
    forget_rows = forget_gate.reshape(head_pairs, 2, length)
    summary = jax.vmap(partial(summarize, block_len=BLOCK))
    queries_one = split_heads(query_one)
    queries_two = split_heads(query_two)
    closing_one, prefix_one, pieces_one = summary(
        queries_one, split_heads(key_one), values_split[:, 0], input_rows[:, 0], forget_rows[:, 0]
    )
    closing_two, prefix_two, pieces_two = summary(
        queries_two, split_heads(key_two), values_split[:, 1], input_rows[:, 1], forget_rows[:, 1]
    )
    identity = (
        empty_state(head_pairs, queries_one.shape[2], width_v),
        empty_state(head_pairs, queries_two.shape[2], width_v),
    )
    incoming = prefix_2((closing_one, closing_two), "sp", combine_groups, identity)
    cell_one = jax.vmap(finish)(queries_one, prefix_one, pieces_one, incoming[0])
    cell_two = jax.vmap(finish)(queries_two, prefix_two, pieces_two, incoming[1])
    normed = jnp.stack([head_norm(cell_one), head_norm(cell_two)], 1)
    normed = normed.transpose(2, 0, 1, 3).reshape(length, 2 * head_pairs * width_v)
    mixed_heads = (normed * head_gain * jax.nn.sigmoid(out_gate.astype(jnp.float32))).astype(
        jnp.bfloat16
    )
    own_rows = length // lax.axis_size("tp")
    leading = lax.axis_index("tp") * own_rows
    up_full, down_full = (
        lax.all_gather(up_weight, "sp", axis=0, tiled=True),
        lax.all_gather(down_weight, "sp", axis=1, tiled=True),
    )
    summed = lax.psum_scatter(
        jnp.dot(mixed_heads, out_weight, preferred_element_type=jnp.float32).astype(jnp.bfloat16),
        "tp",
        scatter_dimension=0,
        tiled=True,
    )
    mixer_out = lax.optimization_barrier(summed)
    stream_own = lax.dynamic_slice_in_dim(stream, leading, own_rows, 0)
    first_own = layer_norm(
        stream_own.astype(jnp.float32) + mixer_out.astype(jnp.float32), mix_gain
    ).astype(jnp.bfloat16)
    hidden = jnp.square(
        jax.nn.relu(
            jnp.dot(
                lax.all_gather(first_own, "tp", axis=0, tiled=True),
                up_full,
                preferred_element_type=jnp.float32,
            )
        )
    ).astype(jnp.bfloat16)
    partial_sums = jnp.dot(hidden, down_full, preferred_element_type=jnp.float32)
    mlp_out = lax.optimization_barrier(
        lax.psum_scatter(partial_sums.astype(jnp.bfloat16), "tp", scatter_dimension=0, tiled=True)
    )
    return layer_norm(first_own.astype(jnp.float32) + mlp_out.astype(jnp.float32), out_gain).astype(
        jnp.bfloat16
    )


def solution(mesh):
    in_specs = (
        P("sp", "tp"),
        P("sp", "tp"),
        P("sp", "tp"),
        P("sp", "tp"),
        P("sp", "tp"),
        P("sp", "tp"),
        P("tp", "sp"),
        P("tp", "sp"),
        P("tp"),
        P("tp", None),
        P("sp", None),
        P(),
        P("sp", "tp"),
        P("tp", "sp"),
        P(),
    )
    out_specs = P(("sp", "tp"), None)
    return jax.shard_map(body, mesh=mesh, in_specs=in_specs, out_specs=out_specs, check_vma=False)
```

profile of v0, /device:TPU:0, one launch (start us, length us, event | category | flops | bytes accessed | tf_op | source)
XLA Modules:
  0.0 683.7 jit_solution(4655088481596444945)
XLA Ops:
  6.6 0.8 fusion.72
  7.5 1.0 reduce_window_sum.18
  8.5 0.1 copy.73
  8.6 0.1 copy.74
  8.7 0.8 fusion.88
  9.5 0.2 fusion.82
  9.8 1.1 reshape.275
  11.0 1.0 copy.76
  12.0 0.2 reshape.290
  12.2 0.2 fusion.53
  12.3 0.3 convolution_bitcast_fusion.3
  12.7 0.7 while.76
  13.4 0.6 copy-done.1
  14.2 1.0 reduce_window_sum.17
  15.3 0.1 copy.65
  15.7 0.2 fusion.81
  16.0 0.1 multiply_reduce_fusion.4
  16.2 0.7 convolution_bitcast_fusion
  16.9 0.8 while.75
  17.0 0.1 fusion.120
  17.4 0.1 fusion.120
  17.7 0.7 copy-done
  18.5 0.1 copy.89
  18.6 0.6 dynamic-slice
  19.7 0.2 dynamic-update-slice.2
  20.0 0.2 dynamic-update-slice.3
  20.2 0.2 dynamic-update-slice
  20.4 0.2 dynamic-update-slice.1
  20.6 43.8 %all-reduce.4 = (f32[64]{0:T(128)S(1)}, f32[64]{0:T(128)S(1)}, f32[64]{0:T(128)S(1)}, f32[64]{0:T(128)S(1)}) all-reduce(f32[64]{0:T(128)S(1)} %dynamic-update-slice, f32[64]{0:T(128)S(1)} %dynamic-update-slice.1, f32[64]{0:T(128)S(1)} %dynamic-update-slice.2, f32[64]{0:T(128)S(1)} %dynamic-update-slice.3), channel_id=2, replica_groups=mesh['sp'=16,'tp'=2] {'sp'}, use_global_device_ids=true, to_apply=%add | all-reduce | flops 256 | bytes 2048
  64.9 0.1 copy.86
  65.0 0.1 reshape.284
  65.1 36.1 %all-gather.9 = f32[16,4,64]{2,1,0:T(4,128)S(1)} all-gather(f32[1,4,64]{2,1,0:T(4,128)S(1)} %bitcast.311), channel_id=9, replica_groups=mesh['sp'=16,'tp'=2] {'sp'}, dimensions={0}, use_global_device_ids=true | all-gather | bytes 17408 | tf_op jit(solution)/shard_map/all_gather | solution.py:14
  101.3 37.9 %all-gather.8 = f32[16,4,128]{2,1,0:T(4,128)S(1)} all-gather(f32[1,4,128]{2,1,0:T(4,128)S(1)} %bitcast.312), channel_id=5, replica_groups=mesh['sp'=16,'tp'=2] {'sp'}, dimensions={0}, use_global_device_ids=true | all-gather | bytes 34816 | tf_op jit(solution)/shard_map/all_gather | solution.py:14
  139.2 0.4 fusion.51
  139.6 15.4 %all-gather.19.cloned.1.call-done = f32[64,128,128]{2,1,0:T(8,128)} async-done(((f32[4,128,128]{2,1,0:T(8,128)}), f32[64,128,128]{2,1,0:T(8,128)}) %all-gather.19.cloned.1.call-update) | async-done | bytes 4194320 | tf_op jit(solution)/shard_map/all_gather | solution.py:14
  155.3 0.3 fusion.69
  155.7 0.4 fusion.91
  156.2 0.5 fusion.35
  156.7 0.5 fusion.92
  157.3 0.3 multiply_reduce_fusion.3
  157.7 0.2 fusion.60
  157.9 0.3 fusion.89
  158.4 0.4 fusion.32
  158.7 0.5 fusion.90
  159.3 0.3 multiply_reduce_fusion.2
  159.7 0.2 fusion.44
  159.9 0.2 fusion.42
  160.2 0.4 copy.92
  160.6 0.4 reshape.286
  161.0 3.8 convolution_convert_fusion.1
  164.9 0.5 all-gather.15.cloned.1.call-update
  165.5 0.5 all-gather.17.cloned.1.call-update
  166.1 39.8 %reduce-scatter.3.cloned.1.call-done = bf16[64,2048]{1,0:T(8,128)(2,1)} async-done(((bf16[128,2048]{1,0:T(8,128)(2,1)}), bf16[64,2048]{1,0:T(8,128)(2,1)}) %reduce-scatter.3.cloned.1.call-update) | async-done | bytes 262160 | tf_op jit(solution)/shard_map/reduce_scatter | solution.py:176
  206.0 1.1 fusion.39
  207.1 1.2 multiply_reduce_fusion.1
  208.3 1.1 multiply_convert_fusion.1
  209.4 2.4 all_gather.73
  211.8 189.0 %all-gather.15.cloned.1.call-done = bf16[2048,4096]{1,0:T(8,128)(2,1)} async-done(((bf16[128,4096]{1,0:T(8,128)(2,1)}), bf16[2048,4096]{1,0:T(8,128)(2,1)}) %all-gather.15.cloned.1.call-update) | async-done | bytes 16777232 | tf_op jit(solution)/shard_map/all_gather | solution.py:173
  400.7 249.9 %all-gather.17.cloned.1.call-done = bf16[4096,2048]{1,0:T(8,128)(2,1)} async-done(((bf16[4096,128]{1,0:T(8,128)(2,1)}), bf16[4096,2048]{1,0:T(8,128)(2,1)}) %all-gather.17.cloned.1.call-update) | async-done | bytes 16777232 | tf_op jit(solution)/shard_map/all_gather | solution.py:174
  650.6 15.9 %convolution_convert_fusion = bf16[128,2048]{1,0:T(8,128)(2,1)} fusion(bf16[4096,2048]{1,0:T(8,128)(2,1)} %all-gather.17.cloned.1.call-done, bf16[128,2048]{1,0:T(8,128)(2,1)S(1)} %all_gather.73, bf16[2048,4096]{1,0:T(8,128)(2,1)} %all-gather.15.cloned.1.call-done), kind=kOutput, calls=%fused_computation.65 | convolution fusion | flops 4296802304 | bytes 34603008 | tf_op jit(solution)/shard_map/dot_general | solution.py:196
  666.5 6.3 reduce-scatter.5.cloned.1.call-done
  672.8 1.1 fusion.41
  673.9 1.2 multiply_reduce_fusion
  675.1 1.8 multiply_convert_fusion
  (141 shorter events, 4.1 us)
Async XLA Ops:
  6.5 9.0 %copy-start.3 = (bf16[128,512]{1,0:T(8,128)(2,1)S(1)}, bf16[128,512]{1,0:T(8,128)(2,1)}, u32[]{:S(2)}) copy-start(bf16[128,512]{1,0:T(8,128)(2,1)} %param.22) | copy-start | bytes 393220
  6.5 133.0 %all-gather.21.cloned.1.call-start = ((), (), s32[]{:S(2)}) async-start(), calls=%async_computation.7 | async-start | bytes 2228224 | tf_op jit(solution)/shard_map/all_gather | solution.py:14
  13.4 0.6 copy-start.1
  14.0 140.9 %all-gather.19.cloned.1.call-start = ((), (), s32[]{:S(2)}) async-start(), calls=%async_computation.6 | async-start | bytes 4456448 | tf_op jit(solution)/shard_map/all_gather | solution.py:14
  16.2 2.4 copy-start.10
  16.2 48.6 %copy-start.4 = (bf16[128,512]{1,0:T(8,128)(2,1)S(1)}, bf16[128,512]{1,0:T(8,128)(2,1)}, u32[]{:S(2)}) copy-start(bf16[128,512]{1,0:T(8,128)(2,1)} %param.21) | copy-start | bytes 393220
  16.9 48.0 %copy-start.5 = (bf16[128,256]{1,0:T(8,128)(2,1)S(1)}, bf16[128,256]{1,0:T(8,128)(2,1)}, u32[]{:S(2)}) copy-start(bf16[128,256]{1,0:T(8,128)(2,1)} %param.23) | copy-start | bytes 196612
  17.7 0.7 copy-start
  18.4 187.6 %reduce-scatter.3.cloned.1.call-start = ((), (), s32[]{:S(2)}) async-start(), calls=%async_computation.2 | async-start | bytes 786432 | tf_op jit(solution)/shard_map/reduce_scatter | solution.py:176
  157.2 3.8 copy-start.8
  157.2 3.8 copy-start.9
  161.0 44.9 %copy-start.2 = (bf16[128,2048]{1,0:T(8,128)(2,1)S(1)}, bf16[128,2048]{1,0:T(8,128)(2,1)}, u32[]{:S(2)}) copy-start(bf16[128,2048]{1,0:T(8,128)(2,1)} %param.31) | copy-start | bytes 1572868
  161.0 47.3 %copy-start.6 = (f32[2048]{0:T(1024)S(1)}, f32[2048]{0:T(1024)}, u32[]{:S(2)}) copy-start(f32[2048]{0:T(1024)} %param.32) | copy-start | bytes 24580
  164.9 235.8 %all-gather.15.cloned.1.call-start = ((), (), s32[]{:S(2)}) async-start(), calls=%async_computation.3 | async-start | bytes 17825792 | tf_op jit(solution)/shard_map/all_gather | solution.py:173
  165.5 485.1 %all-gather.17.cloned.1.call-start = ((), (), s32[]{:S(2)}) async-start(), calls=%async_computation.4 | async-start | bytes 17825792 | tf_op jit(solution)/shard_map/all_gather | solution.py:174
  166.1 506.7 %reduce-scatter.5.cloned.1.call-start = ((), (), s32[]{:S(2)}) async-start(), calls=%async_computation.5 | async-start | bytes 786432 | tf_op jit(solution)/shard_map/reduce_scatter | solution.py:198
  211.8 463.3 %copy-start.7 = (f32[2048]{0:T(1024)S(1)}, f32[2048]{0:T(1024)}, u32[]{:S(2)}) copy-start(f32[2048]{0:T(1024)} %param.35) | copy-start | bytes 24580
Sparse Core Ops, SparseCore 0:
  14.2 63.5 all-gather.20
  80.5 74.4 all-gather.18
  165.0 40.8 reduce-scatter.2
  208.6 192.1 all-gather.14
  403.3 247.2 all-gather.16
  666.6 6.0 reduce-scatter.4
where the time goes:
time: 685 us; the launch traced here: 684 us
  waiting for transfers between devices  501 us (73%)
  blocking collectives  120 us (18%)
  matrix products  23.7 us (3%)
  between operations  14.6 us (2%)
  other arithmetic  13.8 us (2%)
  local copies, waits for them, and re-layouts  9.5 us (1%)
    all_gather x1, waiting for transfers between devices, body(): lax.all_gather(down_weight, 'sp', axis=1, tiled=True)  250 us
    all_gather x1, waiting for transfers between devices, body(): lax.all_gather(up_weight, 'sp', axis=0, tiled=True)  189 us
    all_gather x2, blocking collectives, prefix_2(): gathered = jax.tree.map(lambda a: lax.all_gather(a, axis), part)  74.1 us
    unnamed x1, blocking collectives  43.8 us
    reduce_scatter x1, waiting for transfers between devices, body(): lax.psum_scatter(jnp.dot(mixed_heads, out_weight, preferred_element_type=...  39.8 us
    dot_general x1, matrix products, body(): jnp.dot(hidden, down_full, preferred_element_type=jnp.float32)  15.9 us
    all_gather x2, waiting for transfers between devices, prefix_2(): gathered = jax.tree.map(lambda a: lax.all_gather(a, axis), part)  15.4 us
  transfers between devices with their start and end apart: 6, of which 5 were waited for; matrix products, arithmetic and copies ran while one was open for 1% of the time, Pallas kernels for 0%

commit v1 on v0

--- a/solution.py
+++ b/solution.py
@@ -7,6 +7,14 @@
 BLOCK = 64
 NEG_BIG = -1e30
 EPS = 1e-05
+
+
+def gather_from_all(shard, axis, dim):
+    peers = lax.axis_size(axis)
+    repeats = [peers if d == dim else 1 for d in range(shard.ndim)]
+    return lax.all_to_all(
+        jnp.tile(shard, repeats), axis, split_axis=dim, concat_axis=dim, tiled=True
+    )
 
 
 def prefix_2(part, axis, combine, identity):
@@ -170,7 +178,7 @@
     own_rows = length // lax.axis_size("tp")
     leading = lax.axis_index("tp") * own_rows
     up_full, down_full = (
-        lax.all_gather(up_weight, "sp", axis=0, tiled=True),
+        gather_from_all(up_weight, "sp", 0),
         lax.all_gather(down_weight, "sp", axis=1, tiled=True),
     )
     summed = lax.psum_scatter(

time: 685 us -> 828 us (1.21)
  waiting for transfers between devices: 501 us -> 600 us
  starting transfers between devices: 0.2 us -> 38.9 us
    all_to_all x0 -> x1, waiting for transfers between devices: none -> 368 us  [gather_from_all(): lax.all_to_all(jnp.tile(shard, repeats), axis, split_axis=dim, concat_axi...]
    all_gather x1 -> x0, waiting for transfers between devices: 189 us -> none  [body(): lax.all_gather(up_weight, 'sp', axis=0, tiled=True)]
    all_gather x1, waiting for transfers between devices: 250 us -> 192 us  [body(): lax.all_gather(down_weight, 'sp', axis=1, tiled=True)]
    reduce_scatter x1, waiting for transfers between devices: 39.8 us -> 0.02 us  [body(): lax.psum_scatter(jnp.dot(mixed_heads, out_weight, preferred_element_type=...]
    all_to_all x0 -> x1, starting transfers between devices: none -> 38.8 us  [gather_from_all(): lax.all_to_all(jnp.tile(shard, repeats), axis, split_axis=dim, concat_axi...]
    reduce_scatter x1, waiting for transfers between devices: 6.26 us -> 23.5 us  [body(): lax.psum_scatter(partial_sums.astype(jnp.bfloat16), 'tp', scatter_dimensi...]
  transfers between devices with their start and end apart: 6 -> 6, of which waited for: 5 -> 4; matrix products, arithmetic and copies ran while one was open for 1% -> 2% of each run, Pallas kernels for 0% -> 0%
where the time goes in v1:
time: 828 us; the launch traced here: 826 us
  waiting for transfers between devices  600 us (72%)
  blocking collectives  120 us (14%)
  starting transfers between devices  38.9 us (5%)
  matrix products  23.6 us (3%)
  local copies, waits for them, and re-layouts  15.4 us (2%)
  between operations  14.3 us (2%)
  other arithmetic  13.8 us (2%)
    all_to_all x1, waiting for transfers between devices, gather_from_all(): lax.all_to_all(jnp.tile(shard, repeats), axis, split_axis=dim, concat_axi...  368 us
    all_gather x1, waiting for transfers between devices, body(): lax.all_gather(down_weight, 'sp', axis=1, tiled=True)  192 us
    all_gather x2, blocking collectives, prefix_2(): gathered = jax.tree.map(lambda a: lax.all_gather(a, axis), part)  74.1 us
    unnamed x1, blocking collectives  43.8 us
    all_to_all x1, starting transfers between devices, gather_from_all(): lax.all_to_all(jnp.tile(shard, repeats), axis, split_axis=dim, concat_axi...  38.8 us
    reduce_scatter x1, waiting for transfers between devices, body(): lax.psum_scatter(partial_sums.astype(jnp.bfloat16), 'tp', scatter_dimensi...  23.5 us
  transfers between devices with their start and end apart: 6, of which 4 were waited for; matrix products, arithmetic and copies ran while one was open for 2% of the time, Pallas kernels for 0%

profile of v1, /device:TPU:0, one launch (start us, length us, event | category | flops | bytes accessed | tf_op | source)
XLA Modules:
  0.0 826.3 jit_solution(10255366027202259209)
XLA Ops:
  6.6 0.8 fusion.72
  7.5 1.0 reduce_window_sum.18
  8.5 0.1 copy.73
  8.6 0.1 copy.74
  8.7 0.8 fusion.88
  9.5 0.2 fusion.82
  9.8 1.1 reshape.282
  11.0 1.0 copy.76
  12.0 0.2 reshape.297
  12.2 0.2 fusion.53
  12.3 0.3 convolution_bitcast_fusion.3
  12.7 0.7 while.76
  13.4 0.6 copy-done.1
  14.2 1.0 reduce_window_sum.17
  15.3 0.1 copy.65
  15.7 0.2 fusion.81
  16.0 0.1 multiply_reduce_fusion.4
  16.2 0.7 convolution_bitcast_fusion
  16.9 0.8 while.75
  17.0 0.1 fusion.120
  17.4 0.1 fusion.120
  17.7 0.7 copy-done
  18.5 0.1 copy.89
  18.6 0.6 dynamic-slice
  19.7 0.2 dynamic-update-slice.2
  20.0 0.2 dynamic-update-slice.3
  20.2 0.2 dynamic-update-slice
  20.4 0.2 dynamic-update-slice.1
  20.6 43.8 %all-reduce.4 = (f32[64]{0:T(128)S(1)}, f32[64]{0:T(128)S(1)}, f32[64]{0:T(128)S(1)}, f32[64]{0:T(128)S(1)}) all-reduce(f32[64]{0:T(128)S(1)} %dynamic-update-slice, f32[64]{0:T(128)S(1)} %dynamic-update-slice.1, f32[64]{0:T(128)S(1)} %dynamic-update-slice.2, f32[64]{0:T(128)S(1)} %dynamic-update-slice.3), channel_id=2, replica_groups=mesh['sp'=16,'tp'=2] {'sp'}, use_global_device_ids=true, to_apply=%add | all-reduce | flops 256 | bytes 2048
  64.9 0.1 copy.86
  65.0 0.1 reshape.291
  65.1 36.1 %all-gather.9 = f32[16,4,64]{2,1,0:T(4,128)S(1)} all-gather(f32[1,4,64]{2,1,0:T(4,128)S(1)} %bitcast.312), channel_id=9, replica_groups=mesh['sp'=16,'tp'=2] {'sp'}, dimensions={0}, use_global_device_ids=true | all-gather | bytes 17408 | tf_op jit(solution)/shard_map/all_gather | solution.py:22
  101.3 37.9 %all-gather.8 = f32[16,4,128]{2,1,0:T(4,128)S(1)} all-gather(f32[1,4,128]{2,1,0:T(4,128)S(1)} %bitcast.313), channel_id=5, replica_groups=mesh['sp'=16,'tp'=2] {'sp'}, dimensions={0}, use_global_device_ids=true | all-gather | bytes 34816 | tf_op jit(solution)/shard_map/all_gather | solution.py:22
  139.2 0.4 fusion.51
  139.6 15.4 %all-gather.16.cloned.1.call-done = f32[64,128,128]{2,1,0:T(8,128)} async-done(((f32[4,128,128]{2,1,0:T(8,128)}), f32[64,128,128]{2,1,0:T(8,128)}) %all-gather.16.cloned.1.call-update) | async-done | bytes 4194320 | tf_op jit(solution)/shard_map/all_gather | solution.py:22
  155.3 0.3 fusion.69
  155.7 0.4 fusion.91
  156.2 0.5 fusion.35
  156.7 0.5 fusion.92
  157.3 0.3 multiply_reduce_fusion.3
  157.7 0.2 fusion.60
  157.9 0.3 fusion.89
  158.4 0.4 fusion.32
  158.7 0.5 fusion.90
  159.3 0.3 multiply_reduce_fusion.2
  159.7 0.2 fusion.44
  159.9 0.2 fusion.42
  160.2 0.4 copy.92
  160.6 0.4 reshape.293
  161.0 3.7 convolution_convert_fusion.1
  164.8 6.0 tile.2
  170.8 38.8 %all-to-all-start = ((bf16[16,128,4096]{2,1,0:T(8,128)(2,1)}), bf16[16,128,4096]{2,1,0:T(8,128)(2,1)}, u32[]{:S(2)}, u32[]{:S(2)}) async-start(bf16[16,128,4096]{2,1,0:T(8,128)(2,1)} %tile.2), calls=%async_computation.1 | async-start | bytes 33554432 | tf_op jit(solution)/shard_map/all_to_all | solution.py:15
  209.6 0.5 all-gather.14.cloned.1.call-update
  210.2 1.1 fusion.39
  211.4 1.2 multiply_reduce_fusion.1
  212.6 1.1 multiply_convert_fusion.1
  213.7 2.4 all_gather.70
  216.0 367.9 %all-to-all-done = bf16[16,128,4096]{2,1,0:T(8,128)(2,1)} async-done(((bf16[16,128,4096]{2,1,0:T(8,128)(2,1)}), bf16[16,128,4096]{2,1,0:T(8,128)(2,1)}, u32[]{:S(2)}, u32[]{:S(2)}) %all-to-all-start) | async-done | bytes 16777248 | tf_op jit(solution)/shard_map/all_to_all | solution.py:15
  583.9 192.4 %all-gather.14.cloned.1.call-done = bf16[4096,2048]{1,0:T(8,128)(2,1)} async-done(((bf16[4096,128]{1,0:T(8,128)(2,1)}), bf16[4096,2048]{1,0:T(8,128)(2,1)}) %all-gather.14.cloned.1.call-update) | async-done | bytes 16777232 | tf_op jit(solution)/shard_map/all_gather | solution.py:182
  776.3 15.9 %convolution_convert_fusion = bf16[128,2048]{1,0:T(8,128)(2,1)} fusion(bf16[4096,2048]{1,0:T(8,128)(2,1)} %all-gather.14.cloned.1.call-done, bf16[128,2048]{1,0:T(8,128)(2,1)S(1)} %all_gather.70, bf16[2048,4096]{1,0:T(8,128)(2,1)} %bitcast.57), kind=kOutput, calls=%fused_computation.65 | convolution fusion | flops 4296802304 | bytes 34603008 | tf_op jit(solution)/shard_map/dot_general | solution.py:204
  792.2 23.5 %reduce-scatter.5.cloned.1.call-done = bf16[64,2048]{1,0:T(8,128)(2,1)} async-done(((bf16[128,2048]{1,0:T(8,128)(2,1)}), bf16[64,2048]{1,0:T(8,128)(2,1)}) %reduce-scatter.5.cloned.1.call-update) | async-done | bytes 262160 | tf_op jit(solution)/shard_map/reduce_scatter | solution.py:206
  815.6 1.1 fusion.41
  816.8 1.2 multiply_reduce_fusion
  818.0 1.8 multiply_convert_fusion
  (143 shorter events, 4.0 us)
Async XLA Ops:
  6.5 9.0 %copy-start.4 = (bf16[128,512]{1,0:T(8,128)(2,1)S(1)}, bf16[128,512]{1,0:T(8,128)(2,1)}, u32[]{:S(2)}) copy-start(bf16[128,512]{1,0:T(8,128)(2,1)} %param.22) | copy-start | bytes 393220
  6.5 133.0 %all-gather.18.cloned.1.call-start = ((), (), s32[]{:S(2)}) async-start(), calls=%async_computation.7 | async-start | bytes 2228224 | tf_op jit(solution)/shard_map/all_gather | solution.py:22
  13.4 0.6 copy-start.1
  14.0 140.9 %all-gather.16.cloned.1.call-start = ((), (), s32[]{:S(2)}) async-start(), calls=%async_computation.6 | async-start | bytes 4456448 | tf_op jit(solution)/shard_map/all_gather | solution.py:22
  16.2 2.4 copy-start.11
  16.2 48.6 %copy-start.5 = (bf16[128,512]{1,0:T(8,128)(2,1)S(1)}, bf16[128,512]{1,0:T(8,128)(2,1)}, u32[]{:S(2)}) copy-start(bf16[128,512]{1,0:T(8,128)(2,1)} %param.21) | copy-start | bytes 393220
  16.9 48.0 %copy-start.6 = (bf16[128,256]{1,0:T(8,128)(2,1)S(1)}, bf16[128,256]{1,0:T(8,128)(2,1)}, u32[]{:S(2)}) copy-start(bf16[128,256]{1,0:T(8,128)(2,1)} %param.23) | copy-start | bytes 196612
  17.7 0.7 copy-start
  18.4 191.8 %reduce-scatter.3.cloned.1.call-start = ((), (), s32[]{:S(2)}) async-start(), calls=%async_computation.3 | async-start | bytes 786432 | tf_op jit(solution)/shard_map/reduce_scatter | solution.py:184
  157.2 3.8 copy-start.9
  157.2 3.8 copy-start.10
  160.6 4.2 copy-start.3
  170.8 39.5 %copy-start.2 = (bf16[128,2048]{1,0:T(8,128)(2,1)S(1)}, bf16[128,2048]{1,0:T(8,128)(2,1)}, u32[]{:S(2)}) copy-start(bf16[128,2048]{1,0:T(8,128)(2,1)} %param.31) | copy-start | bytes 1572868
  170.8 41.8 %copy-start.7 = (f32[2048]{0:T(1024)S(1)}, f32[2048]{0:T(1024)}, u32[]{:S(2)}) copy-start(f32[2048]{0:T(1024)} %param.32) | copy-start | bytes 24580
  170.8 413.1 %all-to-all-start = ((bf16[16,128,4096]{2,1,0:T(8,128)(2,1)}), bf16[16,128,4096]{2,1,0:T(8,128)(2,1)}, u32[]{:S(2)}, u32[]{:S(2)}) async-start(bf16[16,128,4096]{2,1,0:T(8,128)(2,1)} %tile.2), calls=%async_computation.1 | async-start | bytes 33554432 | tf_op jit(solution)/shard_map/all_to_all | solution.py:15
  209.6 566.7 %all-gather.14.cloned.1.call-start = ((), (), s32[]{:S(2)}) async-start(), calls=%async_computation.4 | async-start | bytes 17825792 | tf_op jit(solution)/shard_map/all_gather | solution.py:182
  210.1 605.5 %reduce-scatter.5.cloned.1.call-start = ((), (), s32[]{:S(2)}) async-start(), calls=%async_computation.5 | async-start | bytes 786432 | tf_op jit(solution)/shard_map/reduce_scatter | solution.py:206
  776.3 41.7 %copy-start.8 = (f32[2048]{0:T(1024)S(1)}, f32[2048]{0:T(1024)}, u32[]{:S(2)}) copy-start(f32[2048]{0:T(1024)} %param.35) | copy-start | bytes 24580
Sparse Core Ops, SparseCore 0:
  14.2 63.5 all-gather.17
  80.5 74.4 all-gather.15
  164.9 40.8 reduce-scatter.2
  212.8 563.4 all-gather.13
  792.3 23.2 reduce-scatter.4
